TPU v7x, 512 devices: a whole 4x4x16 slice. The times are simulated.
512 devices in a mesh: sp: 16 (over z), fs: 4 (over y), tp: 8 (over x, core).
Axes of the slice: x: 4, y: 4, z: 16, core: 2. Of those that a mesh axis runs over, the one named last changes fastest.
Arguments:
- tokens: bfloat16 [4, 4096, 2048], P('fs', 'sp'), may hold values from -6 to 6
- mix_gain: float32 [2048], replicated, may hold values from 0.1 to 1.9
- query_down: bfloat16 [2048, 768], P('fs', 'tp'), may hold values from -0.125 to 0.125
- memory_down: bfloat16 [2048, 512], P('fs', 'tp'), may hold values from -0.125 to 0.125
- rope_weight: bfloat16 [2048, 32], replicated, may hold values from -0.125 to 0.125
- query_up: bfloat16 [768, 1536], P('fs', 'tp'), may hold values from -0.21875 to 0.21875
- key_up: bfloat16 [512, 1024], P('fs', 'tp'), may hold values from -0.25 to 0.25
- value_up: bfloat16 [512, 1024], P('fs', 'tp'), may hold values from -0.25 to 0.25
- latent_gain: float32 [768], replicated, may hold values from 0.1 to 1.9
- memory_gain: float32 [512], replicated, may hold values from 0.1 to 1.9
- query_gain: float32 [96], replicated, may hold values from 1 to 16
- key_gain: float32 [96], replicated, may hold values from 0.1 to 1.9
- conv_value: bfloat16 [2048, 1024], P('fs', 'tp'), may hold values from -1 to 1
- conv_gate: bfloat16 [2048, 1024], P('fs', 'tp'), may hold values from -0.125 to 0.125
- conv_kernel: bfloat16 [31, 1024], P(None, 'tp'), may hold values from -50 to 50
- channel_gain: float32 [1024], P('tp'), may hold values from 0.1 to 1.9
- channel_shift: float32 [1024], P('tp'), may hold values from -3 to 3
- heads_out: bfloat16 [1024, 2048], P('tp', 'fs'), may hold values from -0.75 to 0.75
- conv_out: bfloat16 [1024, 2048], P('tp', 'fs'), may hold values from -0.1875 to 0.1875
Outputs:
- mixed: bfloat16 [4, 4096, 2048], P('fs', 'sp')
All inputs are finite; a program needn't handle non-finite values.
Results may differ from a plain program's by a relative error of at most 0.015.
The roundings to bfloat16 on the way count: a program that leaves them out, or rounds other values in their place, can miss the bound.
Values may be sent and summed in bfloat16 or wider, within the bound.
A program may use at most 64 MiB of HBM per device.

v0:
```python
import jax
import jax.numpy as jnp
from jax import lax
from jax.sharding import PartitionSpec as P

QK_NOPE = 64
QK_ROPE = 32
V_DIM = 64
CONV_W = 1024
SEG = 64
QK_DIM = 96


epsilon = 1e-06
rope_base = 10000.0
masked_score = -1e30


def side_by_side(arrays, axis, dim, along):
    ends, at = ([], 0)
    for a in arrays[:-1]:
        at += a.shape[along]
        ends.append(at)
    both = jnp.concatenate(arrays, axis=along)
    return tuple(jnp.split(lax.all_gather(both, axis, axis=dim, tiled=True), ends, axis=along))


def laid_out(pieces, dim):
    shape = list(pieces.shape[1:])
    shape[dim] *= pieces.shape[0]
    return jnp.moveaxis(pieces, 0, dim).reshape(shape)


def one_gather(arrays, axis, dims):
    vector = jnp.concatenate([a.reshape(-1) for a in arrays])
    lines, at, outs = (lax.all_gather(vector, axis), 0, [])
    for a, dim in zip(arrays, dims):
        pieces = lines[:, at : at + a.size].reshape(-1, *a.shape)
        outs.append(laid_out(pieces, dim))
        at += a.size
    return tuple(outs)


def from_behind(value, axis, by):
    count = lax.axis_size(axis)
    pairs = [(i, i + by) for i in range(count) if 0 <= i + by < count]
    return lax.ppermute(value, axis, pairs)


def sent_to_all(value, axis):
    copies = jnp.broadcast_to(value, (lax.axis_size(axis), *value.shape))
    return lax.all_to_all(copies, axis, split_axis=0, concat_axis=0, tiled=True)


def over_copies(value, axis):
    everything = sent_to_all(value, axis)
    return jnp.sum(everything, axis=0)


def packed_total(arrays, axis):
    vector, at, outs = (jnp.concatenate([a.reshape(-1) for a in arrays]), 0, [])
    total = over_copies(vector, axis)
    for a in arrays:
        outs.append(total[at : at + a.size].reshape(a.shape))
        at += a.size
    return tuple(outs)


def over_pieces(value, axis):
    return lax.all_gather(value, axis).astype(jnp.float32).sum(0)


def norm_rows(matrix, scale_vector):
    return (
        matrix
        * lax.rsqrt(jnp.mean(matrix * matrix, axis=-1, keepdims=True) + epsilon)
        * scale_vector
    )


def rope_tables(positions):
    inverse_freq = 1.0 / rope_base ** (jnp.arange(0, QK_ROPE, 2, dtype=jnp.float32) / QK_ROPE)
    angles = positions.astype(jnp.float32)[:, None] * inverse_freq[None, :]
    return (jnp.cos(angles)[:, None, :], jnp.sin(angles)[:, None, :])


def rotate(matrix, cosine_table, sine_table):
    half_width = matrix.shape[-1] // 2
    front_half = matrix[..., :half_width]
    back_half = matrix[..., half_width:]
    return jnp.concatenate(
        [
            front_half * cosine_table - back_half * sine_table,
            front_half * sine_table + back_half * cosine_table,
        ],
        axis=-1,
    )


def heads_query(latent, weight, scale_vector, cosine_table, sine_table):
    row_count = latent.shape[0]
    projected = jnp.dot(latent, weight, preferred_element_type=jnp.float32)
    projected = norm_rows(
        projected.reshape(row_count, weight.shape[1] // QK_DIM, QK_DIM), scale_vector
    )
    turned = rotate(projected[..., QK_NOPE:], cosine_table, sine_table)
    return jnp.concatenate([projected[..., :QK_NOPE], turned], axis=-1).astype(jnp.bfloat16)


def heads_key(latent, rope_rows, weight, scale_vector, cosine_table, sine_table):
    row_count = latent.shape[0]
    head_count = weight.shape[1] // QK_NOPE
    nope_part = jnp.dot(latent, weight, preferred_element_type=jnp.float32).reshape(
        row_count, head_count, QK_NOPE
    )
    shared = jnp.broadcast_to(
        rope_rows.astype(jnp.float32)[:, None, :], (row_count, head_count, QK_ROPE)
    )
    joined = norm_rows(jnp.concatenate([nope_part, shared], axis=-1), scale_vector)
    turned = rotate(joined[..., QK_NOPE:], cosine_table, sine_table)
    return jnp.concatenate([joined[..., :QK_NOPE], turned], axis=-1).astype(jnp.bfloat16)


def depthwise(extended, kernel, row_count):

    def add_tap(tap_index, running):
        window = lax.dynamic_slice_in_dim(extended, tap_index, row_count, 0).astype(jnp.float32)
        weight_row = lax.dynamic_slice_in_dim(kernel, tap_index, 1, 0).astype(jnp.float32)
        return running + window * weight_row

    return lax.fori_loop(
        0, kernel.shape[0], add_tap, jnp.zeros((row_count, kernel.shape[1]), jnp.float32)
    )


def key_block(key_count):
    block_size = key_count
    while block_size > 2048 and block_size % 2 == 0:
        block_size = block_size // 2
    return block_size


def local(
    tokens,
    mix_gain,
    query_down,
    memory_down,
    rope_weight,
    query_up,
    key_up,
    value_up,
    latent_gain,
    memory_gain,
    query_gain,
    key_gain,
    conv_value,
    conv_gate,
    conv_kernel,
    channel_gain,
    channel_shift,
    heads_out,
    conv_out,
):
    own_rows = tokens[0]
    normed = norm_rows(own_rows.astype(jnp.float32), mix_gain).astype(jnp.bfloat16)
    down_query, down_memory, conv_values, conv_gates, up_query, up_keys, up_values = (
        *side_by_side((query_down, memory_down, conv_value, conv_gate), "fs", 0, 1),
        lax.all_gather(query_up, "fs", axis=0, tiled=True),
        *side_by_side((key_up, value_up), "fs", 0, 1),
    )
    out_heads, out_conv = side_by_side((heads_out, conv_out), "fs", 1, 0)
    joined = jnp.concatenate(
        [down_query, down_memory, rope_weight, conv_values, conv_gates], axis=1
    )
    query_cols = down_query.shape[1]
    memory_cols = down_memory.shape[1]
    conv_cols = conv_values.shape[1]
    projected = jnp.dot(normed, joined, preferred_element_type=jnp.float32)
    row_count = projected.shape[0]
    rope_start = query_cols + memory_cols
    value_start = rope_start + QK_ROPE
    latent_query = projected[:, :query_cols].astype(jnp.bfloat16)
    latent_memory = projected[:, query_cols:rope_start].astype(jnp.bfloat16)
    rope_rows = projected[:, rope_start:value_start].astype(jnp.bfloat16)
    gated = (
        projected[:, value_start : value_start + conv_cols]
        * jax.nn.sigmoid(projected[:, value_start + conv_cols :])
    ).astype(jnp.bfloat16)
    whole_query, whole_memory = one_gather((latent_query, latent_memory), "tp", (1, 1))
    query_normed = norm_rows(whole_query.astype(jnp.float32), latent_gain).astype(jnp.bfloat16)
    memory_normed = norm_rows(whole_memory.astype(jnp.float32), memory_gain).astype(jnp.bfloat16)
    positions = lax.axis_index("sp") * row_count + jnp.arange(row_count, dtype=jnp.int32)
    cosine_table, sine_table = rope_tables(positions)
    queries = heads_query(query_normed, up_query, query_gain, cosine_table, sine_table)
    head_count = queries.shape[1]
    query_segment = positions // SEG
    score_scale = QK_DIM ** (-0.5)
    tap_count = conv_kernel.shape[0]
    left_rim = from_behind(gated[row_count - (tap_count - 1) :], "sp", 1)
    conv_sum = depthwise(jnp.concatenate([left_rim, gated], axis=0), conv_kernel, row_count)
    row_sums, row_squares = packed_total(
        (jnp.sum(conv_sum, axis=1), jnp.sum(conv_sum * conv_sum, axis=1)), "tp"
    )
    row_mean = row_sums / CONV_W
    spread = row_squares / CONV_W - row_mean * row_mean
    centered = conv_sum - row_mean[:, None]
    conv_result = jax.nn.silu(
        centered * lax.rsqrt(spread[:, None] + epsilon) * channel_gain + channel_shift
    ).astype(jnp.bfloat16)

    def attend(state_carry, key_rows, value_rows, key_pos):
        running_max, row_total, weighted = state_carry
        scores = (
            jnp.einsum("qhd,khd->qhk", queries, key_rows, preferred_element_type=jnp.float32)
            * score_scale
        )
        allowed = ((key_pos // SEG)[None, :] <= query_segment[:, None])[:, None, :]
        scores = jnp.where(allowed, scores, masked_score)
        new_max = jnp.maximum(running_max, jnp.max(scores, axis=2))
        weights = jnp.where(allowed, jnp.exp(scores - new_max[:, :, None]), 0.0)
        factor = jnp.exp(running_max - new_max)
        row_total = row_total * factor + jnp.sum(weights, axis=2)
        weighted = weighted * factor[:, :, None] + jnp.einsum(
            "qhk,khd->qhd",
            weights.astype(jnp.bfloat16),
            value_rows,
            preferred_element_type=jnp.float32,
        )
        return (new_max, row_total, weighted)

    initial = (
        jnp.full((row_count, head_count), masked_score, jnp.float32),
        jnp.zeros((row_count, head_count), jnp.float32),
        jnp.zeros((row_count, head_count, V_DIM), jnp.float32),
    )
    own_keys = heads_key(
        memory_normed, rope_rows, up_keys, key_gain, cosine_table, sine_table
    ).reshape(row_count, head_count * QK_DIM)
    own_values = jnp.dot(memory_normed, up_values, preferred_element_type=jnp.float32).astype(
        jnp.bfloat16
    )
    key_piece, value_piece = side_by_side((own_keys, own_values), "sp", 0, 1)

    def block_keys(block_start, block_size):
        key_rows = lax.dynamic_slice_in_dim(key_piece, block_start, block_size, 0).reshape(
            block_size, head_count, QK_DIM
        )
        value_rows = lax.dynamic_slice_in_dim(value_piece, block_start, block_size, 0).reshape(
            block_size, head_count, V_DIM
        )
        key_pos = block_start + jnp.arange(block_size, dtype=jnp.int32)
        return (key_rows, value_rows, key_pos)

    key_count = key_piece.shape[0]
    block_size = key_block(key_count)

    def step(block_index, running):
        key_rows, value_rows, key_pos = block_keys(block_index * block_size, block_size)
        return attend(running, key_rows, value_rows, key_pos)

    final_state = lax.fori_loop(0, key_count // block_size, step, initial)
    running_max, row_total, weighted = final_state
    attention = (
        (weighted / row_total[:, :, None])
        .astype(jnp.bfloat16)
        .reshape(row_count, head_count * V_DIM)
    )
    mixer_rows = jnp.concatenate([attention, conv_result], axis=1)
    out_weight = jnp.concatenate([out_heads, out_conv], axis=0)
    partial_sum = jnp.dot(mixer_rows, out_weight, preferred_element_type=jnp.float32)
    mixed = over_pieces(partial_sum.astype(jnp.bfloat16), "tp").astype(jnp.float32)
    return mixed.astype(jnp.bfloat16)[None]


def solution(mesh):
    in_specs = (
        P("fs", "sp", None),
        P(),
        P("fs", "tp"),
        P("fs", "tp"),
        P(),
        P("fs", "tp"),
        P("fs", "tp"),
        P("fs", "tp"),
        P(),
        P(),
        P(),
        P(),
        P("fs", "tp"),
        P("fs", "tp"),
        P(None, "tp"),
        P("tp"),
        P("tp"),
        P("tp", "fs"),
        P("tp", "fs"),
    )
    out_specs = P("fs", "sp", None)
    return jax.shard_map(local, mesh=mesh, in_specs=in_specs, out_specs=out_specs, check_vma=False)
```

profile of v0, /device:TPU:1, one launch (start us, length us, event | category | flops | bytes accessed | tf_op | source)
XLA Modules:
  0.0 266.6 jit_solution(5219154865961062994)
XLA Ops:
  6.5 1.1 copy.74
  7.6 1.0 copy.75
  8.6 2.1 pad_maximum_fusion
  10.8 1.9 copy.76
  13.4 0.8 pad_maximum_fusion.8
  14.2 10.7 %all_gather.30 = bf16[512,256]{1,0:T(8,128)(2,1)S(1)} all-gather(bf16[128,256]{1,0:T(8,128)(2,1)S(1)} %pad_maximum_fusion.8), channel_id=1, replica_groups=mesh['sp'=16,'fs'=4,'tp'=8] {'fs'}, dimensions={0}, use_global_device_ids=true | all-gather | bytes 327680 | tf_op jit(solution)/shard_map/all_gather | solution.py:25
  25.8 0.8 mul.347
  26.5 9.8 %all_gather.32 = bf16[768,192]{1,0:T(8,128)(2,1)S(1)} all-gather(bf16[192,192]{1,0:T(8,128)(2,1)} %param.28), channel_id=1, replica_groups=mesh['sp'=16,'fs'=4,'tp'=8] {'fs'}, dimensions={0}, use_global_device_ids=true | all-gather | bytes 368640 | tf_op jit(solution)/shard_map/all_gather | solution.py:168
  37.0 19.0 %all-gather.7.cloned.1.call-done = bf16[2048,416]{1,0:T(8,128)(2,1)} async-done(((bf16[512,416]{1,0:T(8,128)(2,1)}), bf16[2048,416]{1,0:T(8,128)(2,1)}) %all-gather.7.cloned.1.call-update) | async-done | bytes 1703952 | tf_op jit(solution)/shard_map/all_gather | solution.py:25
  56.0 2.0 split.29
  58.0 2.7 %fusion.51 = (bf16[256,448]{0,1:T(8,128)(2,1)S(1)}, f32[256,448]{0,1:T(8,128)}) fusion(bf16[2048,256]{1,0:T(8,128)(2,1)S(1)} %split.29, bf16[2048,32]{1,0:T(8,128)(2,1)S(1)} %copy-done.4, bf16[2048,160]{1,0:T(8,128)(2,1)S(1)} %slice-done.1, bf16[1,256,2048]{2,1,0:T(8,128)(2,1)S(1)} %copy-done.3, f32[2048]{0:T(1024)S(1)} %copy-done.9, ...), kind=kOutput, calls=%fused_computation.114 | convolution fusion | flops 477478912 | bytes 3580928 | tf_op jit(solution)/shard_map/dot_general | solution.py:178
  61.2 13.9 %all-gather = bf16[327680]{0:T(1024)(128)(2,1)S(1)} all-gather(bf16[40960]{0:T(1024)(128)(2,1)S(1)} %pad_maximum_fusion.7), channel_id=2, replica_groups=mesh['sp'=16,'fs'=4,'tp'=8] {'tp'}, dimensions={0}, use_global_device_ids=true | all-gather | bytes 737280 | tf_op jit(solution)/shard_map/all_gather | solution.py:36
  78.2 0.8 multiply_multiply_fusion
  80.5 1.0 fusion.47
  81.6 2.9 %collective-permute-start = (bf16[30,128]{0,1:T(8,128)(2,1)S(1)}, bf16[30,128]{0,1:T(8,128)(2,1)S(1)}, u32[]{:S(2)}, u32[]{:S(2)}) collective-permute-start(bf16[30,128]{0,1:T(8,128)(2,1)S(1)} %slice.91), channel_id=1, source_target_pairs={{0,32},{32,64},{64,96},{96,128},{128,160},{160,192},{192,224},{224... | collective-permute-start | bytes 23048 | tf_op jit(solution)/shard_map/ppermute | solution.py:47
  84.6 1.6 pad_maximum_fusion.1
  86.4 30.1 %while.35 = (s32[]{:T(128)}, f32[256,128]{1,0:T(8,128)S(1)}, bf16[286,128]{0,1:T(8,128)(2,1)S(1)}, bf16[31,128]{1,0:T(8,128)(2,1)}, s32[]{:T(128)}, /*index=5*/s32[]{:T(128)}) while((s32[]{:T(128)}, f32[256,128]{1,0:T(8,128)S(1)}, bf16[286,128]{0,1:T(8,128)(2,1)S(1)}, bf16[31,128]{1,0:T(8,128)(2,1)}, s32[]{:T(128)}, ...), condition=%wide.region_10.11_spmd.clone, body=%wide.region_9.10_spmd.clone.sunk | while | flops 131203 | bytes 591191 | solution.py:131
  117.3 4.1 %all-to-all-start = ((f32[8,1,512]{2,1,0:T(1,128)}), f32[8,1,512]{2,1,0:T(1,128)S(1)}, u32[]{:S(2)}, u32[]{:S(2)}) async-start(f32[8,1,512]{2,1,0:T(1,128)} %broadcast_in_dim.109), calls=%async_computation | async-start | bytes 32768 | tf_op jit(solution)/shard_map/all_to_all | solution.py:52
  121.5 4.5 %all-to-all-done = f32[8,1,512]{2,1,0:T(1,128)S(1)} async-done(((f32[8,1,512]{2,1,0:T(1,128)}), f32[8,1,512]{2,1,0:T(1,128)S(1)}, u32[]{:S(2)}, u32[]{:S(2)}) %all-to-all-start) | async-done | bytes 16416 | tf_op jit(solution)/shard_map/all_to_all | solution.py:52
  126.2 25.2 %all-gather.9.cloned.1.call-done = bf16[4096,320]{0,1:T(8,128)(2,1)} async-done(((bf16[256,320]{0,1:T(8,128)(2,1)}), bf16[4096,320]{0,1:T(8,128)(2,1)}) %all-gather.9.cloned.1.call-update) | async-done | bytes 2621456 | tf_op jit(solution)/shard_map/all_gather | solution.py:25
  151.5 1.6 split.32
  153.2 16.1 %while.34 = (s32[]{:T(128)}, f32[256,2]{0,1:T(2,128)S(1)}, f32[256,2]{0,1:T(2,128)S(1)}, f32[256,2,64]{0,2,1:T(8,128)S(1)}, bf16[4096,192]{0,1:T(8,128)(2,1)S(1)...) while((s32[]{:T(128)}, f32[256,2]{0,1:T(2,128)S(1)}, ...), condition=%wide.region_8.9_spmd.clone, body=%wide.region_5.0_spmd.clone.sunk | while | flops 349837824 | bytes 35801304 | solution.py:261
  153.7 2.8 %fusion.75 = (f32[256,2]{0,1:T(2,128)S(1)}, f32[2,2048,256]{2,1,0:T(8,128)}) fusion(pred[256,2048]{0,1:T(8,128)(4,1)S(1)} %broadcast_compare_fusion.2, bf16[2048,2,96]{0,2,1:T(8,128)(2,1)S(1)} %bitcast.88, bf16[256,2,96]{0,2,1:T(8,128)(2,1)S(1)} %get-tuple-element.527), kind=kOutput, calls=%fused_computation.3.clone.1 | convolution fusion | flops 204471808 | bytes 5605376 | tf_op jit(solution)/shard_map/while/body/eval_jaxpr/qhd,khd->qhk/dot_general | solution.py:214
  156.6 3.4 %fusion.77 = f32[256,2]{0,1:T(2,128)S(1)} fusion(f32[2,2048,256]{2,1,0:T(8,128)} %get-tuple-element.473, f32[256,2]{0,1:T(2,128)S(1)} %fusion.76, pred[256,2048]{0,1:T(8,128)(4,1)S(1)} %broadcast_compare_fusion.2), kind=kLoop, calls=%fused_computation.5.clone.1 | loop fusion | flops 5242368 | bytes 4722688 | tf_op jit(solution)/shard_map/while/body/eval_jaxpr/reduce_sum | solution.py:222
  160.1 1.1 fusion.79
  161.8 2.8 %fusion.75 = (f32[256,2]{0,1:T(2,128)S(1)}, f32[2,2048,256]{2,1,0:T(8,128)}) fusion(pred[256,2048]{0,1:T(8,128)(4,1)S(1)} %broadcast_compare_fusion.2, bf16[2048,2,96]{0,2,1:T(8,128)(2,1)S(1)} %bitcast.88, bf16[256,2,96]{0,2,1:T(8,128)(2,1)S(1)} %get-tuple-element.527), kind=kOutput, calls=%fused_computation.3.clone.1 | convolution fusion | flops 204471808 | bytes 5605376 | tf_op jit(solution)/shard_map/while/body/eval_jaxpr/qhd,khd->qhk/dot_general | solution.py:214
  164.6 3.4 %fusion.77 = f32[256,2]{0,1:T(2,128)S(1)} fusion(f32[2,2048,256]{2,1,0:T(8,128)} %get-tuple-element.473, f32[256,2]{0,1:T(2,128)S(1)} %fusion.76, pred[256,2048]{0,1:T(8,128)(4,1)S(1)} %broadcast_compare_fusion.2), kind=kLoop, calls=%fused_computation.5.clone.1 | loop fusion | flops 5242368 | bytes 4722688 | tf_op jit(solution)/shard_map/while/body/eval_jaxpr/reduce_sum | solution.py:222
  168.2 1.1 fusion.79
  169.3 21.4 %all-gather.11.cloned.1.call-done = bf16[256,2048]{1,0:T(8,128)(2,1)} async-done(((bf16[256,512]{1,0:T(8,128)(2,1)}), bf16[256,2048]{1,0:T(8,128)(2,1)}) %all-gather.11.cloned.1.call-update) | async-done | bytes 1048592 | tf_op jit(solution)/shard_map/all_gather | solution.py:25
  190.7 2.7 convolution_convert_fusion
  193.4 60.4 %all-gather.13.cloned.1.call-done = bf16[2048,2048]{1,0:T(8,128)(2,1)} async-done(((bf16[256,2048]{1,0:T(8,128)(2,1)}), bf16[2048,2048]{1,0:T(8,128)(2,1)}) %all-gather.13.cloned.1.call-update) | async-done | bytes 8388624 | tf_op jit(solution)/shard_map/all_gather | solution.py:70
  253.7 6.4 %reduce_sum.108 = bf16[256,2048]{1,0:T(8,128)(2,1)} reduce(bf16[8,256,2048]{2,1,0:T(8,128)(2,1)} %bitcast.91, bf16[]{:T(256)} %constant.206.clone.1), dimensions={0}, to_apply=%region_14.15 | reduce | flops 3670016 | bytes 9437186 | tf_op jit(solution)/shard_map/reduce_sum | solution.py:70
  (234 shorter events, 38.9 us)
Async XLA Ops:
  6.5 30.0 %copy-start.3 = (bf16[1,256,2048]{2,1,0:T(8,128)(2,1)S(1)}, bf16[1,256,2048]{2,1,0:T(8,128)(2,1)}, u32[]{:S(2)}) copy-start(bf16[1,256,2048]{2,1,0:T(8,128)(2,1)} %param.23) | copy-start | bytes 3145732
  6.5 49.5 %all-gather.7.cloned.1.call-start = ((), (), s32[]{:S(2)}) async-start(), calls=%async_computation.1 | async-start | bytes 2621440 | tf_op jit(solution)/shard_map/all_gather | solution.py:25
  10.7 47.3 %copy-start.9 = (f32[2048]{0:T(1024)S(1)}, f32[2048]{0:T(1024)}, u32[]{:S(2)}) copy-start(f32[2048]{0:T(1024)} %param.24) | copy-start | bytes 24580
  10.7 140.8 %all-gather.9.cloned.1.call-start = ((), (), s32[]{:S(2)}) async-start(), calls=%async_computation.2 | async-start | bytes 2785280 | tf_op jit(solution)/shard_map/all_gather | solution.py:25
  24.9 0.7 copy-start.1
  56.0 2.0 slice-start.1
  56.0 2.0 copy-start.4
  76.8 2.5 copy-start.6
  77.3 2.2 copy-start.2
  77.5 7.1 %copy-start.5 = (bf16[128,512]{1,0:T(8,128)(2,1)S(1)}, bf16[128,512]{1,0:T(8,128)(2,1)}, u32[]{:S(2)}) copy-start(bf16[128,512]{1,0:T(8,128)(2,1)} %param.41) | copy-start | bytes 393220
  79.0 47.1 %copy-start.7 = (f32[128]{0:T(128)S(1)}, f32[128]{0:T(128)}, u32[]{:S(2)}) copy-start(f32[128]{0:T(128)} %param.39) | copy-start | bytes 1540
  79.0 47.1 %copy-start.8 = (f32[128]{0:T(128)S(1)}, f32[128]{0:T(128)}, u32[]{:S(2)}) copy-start(f32[128]{0:T(128)} %param.38) | copy-start | bytes 1540
  80.5 110.2 %all-gather.11.cloned.1.call-start = ((), (), s32[]{:S(2)}) async-start(), calls=%async_computation.3 | async-start | bytes 1310720 | tf_op jit(solution)/shard_map/all_gather | solution.py:25
  81.6 4.7 %collective-permute-start = (bf16[30,128]{0,1:T(8,128)(2,1)S(1)}, bf16[30,128]{0,1:T(8,128)(2,1)S(1)}, u32[]{:S(2)}, u32[]{:S(2)}) collective-permute-start(bf16[30,128]{0,1:T(8,128)(2,1)S(1)} %slice.91), channel_id=1, source_target_pairs={{0,32},{32,64},{64,96},{96,128},{128,160},{160,192},{192,224},{224... | collective-permute-start | bytes 23048 | tf_op jit(solution)/shard_map/ppermute | solution.py:47
  117.3 8.8 %all-to-all-start = ((f32[8,1,512]{2,1,0:T(1,128)}), f32[8,1,512]{2,1,0:T(1,128)S(1)}, u32[]{:S(2)}, u32[]{:S(2)}) async-start(f32[8,1,512]{2,1,0:T(1,128)} %broadcast_in_dim.109), calls=%async_computation | async-start | bytes 32768 | tf_op jit(solution)/shard_map/all_to_all | solution.py:52
  121.4 132.3 %all-gather.13.cloned.1.call-start = ((), (), s32[]{:S(2)}) async-start(), calls=%async_computation.4 | async-start | bytes 9437184 | tf_op jit(solution)/shard_map/all_gather | solution.py:70
  151.5 1.7 slice-start
  156.6 3.5 %copy-start = (f32[2,2048,256]{2,1,0:T(8,128)S(1)}, f32[2,2048,256]{2,1,0:T(8,128)}, u32[]{:S(2)}) copy-start(f32[2,2048,256]{2,1,0:T(8,128)} %get-tuple-element.473) | copy-start | bytes 12582916 | tf_op jit(solution)/shard_map/while
  164.6 3.5 %copy-start = (f32[2,2048,256]{2,1,0:T(8,128)S(1)}, f32[2,2048,256]{2,1,0:T(8,128)}, u32[]{:S(2)}) copy-start(f32[2,2048,256]{2,1,0:T(8,128)} %get-tuple-element.473) | copy-start | bytes 12582916 | tf_op jit(solution)/shard_map/while
Sparse Core Ops, SparseCore 0:
  10.8 45.1 all-gather.6
  80.6 70.8 all-gather.8
  153.6 37.0 all-gather.10
  193.5 60.1 all-gather.12
where the time goes:
time: 268 us; the launch traced here: 267 us
  waiting for transfers between devices  131 us (49%)
  other arithmetic  46.1 us (17%)
  blocking collectives  34.5 us (13%)
  local copies, waits for them, and re-layouts  19.8 us (7%)
  matrix products  13.8 us (5%)
  between operations  13.6 us (5%)
  starting transfers between devices  7.13 us (3%)
    all_gather x3, waiting for transfers between devices, side_by_side(): lax.all_gather(both, axis, axis=dim, tiled=True)  65.6 us
    all_gather x1, waiting for transfers between devices, over_pieces(): return lax.all_gather(value, axis).astype(jnp.float32).sum(0)  60.4 us
    mul x31, other arithmetic, add_tap(): return running + window * weight_row  21.5 us
    all_gather x1, blocking collectives, one_gather(): lines, at, outs = (lax.all_gather(vector, axis), 0, [])  13.9 us
    all_gather x1, blocking collectives, side_by_side(): lax.all_gather(both, axis, axis=dim, tiled=True)  10.7 us
    all_gather x1, blocking collectives, local(): lax.all_gather(query_up, 'fs', axis=0, tiled=True)  9.83 us
    reduce_sum x2, other arithmetic, attend(): row_total = row_total * factor + jnp.sum(weights, axis=2)  6.89 us
    reduce_sum x1, other arithmetic, over_pieces(): return lax.all_gather(value, axis).astype(jnp.float32).sum(0)  6.39 us
  transfers between devices with their start and end apart: 6, of which 5 were waited for; matrix products, arithmetic and copies ran while one was open for 21% of the time, Pallas kernels for 0%

commit v1 on v0

v1 whole, which is shorter than its diff:
```python
import functools
import math

import jax
import jax.numpy as jnp
from jax import lax
from jax.experimental import pallas as pl
from jax.experimental.pallas import tpu as pltpu
from jax.sharding import PartitionSpec as P

D = 2048
ROWS = 256
QK_NOPE = 64
QK_ROPE = 32
QK_DIM = 96
V_DIM = 64
Q_LAT = 768
KV_LAT = 512
CONV_W = 1024
CONV_K = 31
SEG = 64
N_SP = 16
N_FS = 4
N_TP = 8
HEAD_ROWS = QK_DIM + V_DIM

epsilon = 1e-06
rope_base = 10000.0
masked_score = -1e30
score_scale = QK_DIM**-0.5 * math.log2(math.e)

F32 = jnp.float32
BF16 = jnp.bfloat16


def remote(src, dst, send, recv, **where):
    return pltpu.make_async_remote_copy(
        src_ref=src,
        dst_ref=dst,
        send_sem=send,
        recv_sem=recv,
        device_id=where,
        device_id_type=pl.DeviceIdType.MESH,
    )


def dot(a, b, contract=(1, 0)):
    return lax.dot_general(
        a, b, (((contract[0],), (contract[1],)), ((), ())), preferred_element_type=F32
    )


def column(row, width):
    n = row.shape[1]
    tall = jnp.broadcast_to(row, (128, n)).T
    return jnp.concatenate([tall] * (width // 128), axis=1)


def turned(block, cosine, sine):
    a, b = block[:16], block[16:]
    return jnp.concatenate([a * cosine - b * sine, a * sine + b * cosine], axis=0)


def kernel(
    tokens_h, md_h, qd_h, qu_h, ku_h, vu_h, cv_h, cg_h, ho_h, co_h,
    mix_gain, rope_weight, latent_gain, memory_gain, query_gain, key_gain,
    conv_kernel, channel_gain, channel_shift, tables,
    out_h,
    tok, nrm, MD, KVU, QD, QU, CV, HC, LM, LQ, KV, qt, stat, halo, ext, cmix,
    sm_max, sm_sum, sm_acc, part, pair_in, total, r1, s2, r2, outv,
    load_sem, ys, yr, ts, tr, zs, zr, hs, hr, ds, dr, xs, xr, out_sem,
):
    z = lax.axis_index("sp")
    f = lax.axis_index("fs")
    t = lax.axis_index("tp")
    x = t // 2
    core = t % 2

    loads = []

    def load(src, dst):
        copy = pltpu.make_async_copy(src, dst, load_sem.at[len(loads)])
        copy.start()
        loads.append(copy)
        return len(loads) - 1

    load(md_h, MD.at[f])
    load(tokens_h.at[0], tok)
    load(ku_h, KVU.at[f, :, pl.ds(0, 128)])
    load(vu_h, KVU.at[f, :, pl.ds(128, 128)])
    load(qd_h, QD.at[f])
    load(qu_h, QU.at[f])
    load(cv_h, CV.at[f, :, pl.ds(0, 128)])
    load(cg_h, CV.at[f, :, pl.ds(128, 128)])
    load(ho_h, HC.at[f, pl.ds(0, 128)])
    load(co_h, HC.at[f, pl.ds(128, 128)])

    barrier = pltpu.get_barrier_semaphore()
    for d in range(1, N_FS):
        pl.semaphore_signal(
            barrier, inc=1, device_id={"fs": (f + d) % N_FS}, device_id_type=pl.DeviceIdType.MESH
        )
    for d in range(1, N_TP):
        pl.semaphore_signal(
            barrier, inc=1, device_id={"tp": (t + d) % N_TP}, device_id_type=pl.DeviceIdType.MESH
        )
    for d in (1, N_SP - 1):
        pl.semaphore_signal(
            barrier, inc=1, device_id={"sp": (z + d) % N_SP}, device_id_type=pl.DeviceIdType.MESH
        )
    pl.semaphore_wait(barrier, N_FS - 1 + N_TP - 1 + 2)

    up, down = (f + 1) % N_FS, (f + N_FS - 1) % N_FS
    far = (f + 2) % N_FS
    weights = [MD, KVU, QD, QU, CV, HC]

    def y_copies(i):
        buf = weights[i]
        half = buf.shape[1] // 2
        top, low = pl.ds(0, half), pl.ds(half, half)
        own_up = remote(buf.at[f], buf.at[f], ys.at[i, 0], yr.at[i, 0], fs=up)
        own_down = remote(buf.at[f], buf.at[f], ys.at[i, 1], yr.at[i, 1], fs=down)
        fwd_up = remote(buf.at[down, top], buf.at[down, top], ys.at[i, 2], yr.at[i, 2], fs=up)
        fwd_down = remote(buf.at[up, low], buf.at[up, low], ys.at[i, 3], yr.at[i, 3], fs=down)
        in_down = remote(buf.at[down], buf.at[down], ys.at[i, 0], yr.at[i, 0], fs=up)
        in_up = remote(buf.at[up], buf.at[up], ys.at[i, 1], yr.at[i, 1], fs=down)
        in_far_top = remote(buf.at[far, top], buf.at[far, top], ys.at[i, 2], yr.at[i, 2], fs=up)
        in_far_low = remote(buf.at[far, low], buf.at[far, low], ys.at[i, 3], yr.at[i, 3], fs=down)
        return own_up, own_down, fwd_up, fwd_down, in_down, in_up, in_far_top, in_far_low

    def y_send(i):
        c = y_copies(i)
        c[0].start()
        c[1].start()

    def y_forward(i):
        c = y_copies(i)
        c[4].wait_recv()
        c[2].start()
        c[5].wait_recv()
        c[3].start()

    def y_finish(i):
        c = y_copies(i)
        c[6].wait_recv()
        c[7].wait_recv()

    def tp_send(k, buf):
        def body(d, _):
            remote(buf.at[t], buf.at[t], ts.at[k, d], tr.at[k, d], tp=(t + d) % N_TP).start()
            return 0

        lax.fori_loop(1, N_TP, body, 0)

    def tp_wait(k, buf):
        def body(d, _):
            src = (t + N_TP - d) % N_TP
            remote(buf.at[src], buf.at[src], ts.at[k, d], tr.at[k, d], tp=src).wait_recv()
            return 0

        lax.fori_loop(1, N_TP, body, 0)

    ahead, behind = (z + 1) % N_SP, (z + N_SP - 1) % N_SP

    def z_copy(way, step, h, slot):
        piece = KV.at[slot, pl.ds(h * HEAD_ROWS, HEAD_ROWS)]
        return remote(
            piece, piece, zs.at[way, step, h], zr.at[way, step, h], sp=ahead if way == 0 else behind
        )

    def attend(slot, own):
        def one_head(h, _):
            keys = KV[slot, pl.ds(h * HEAD_ROWS, QK_DIM), :]
            vals = KV[slot, pl.ds(h * HEAD_ROWS + QK_DIM, V_DIM), :]
            s = dot(keys, qt[h], (0, 0)) * score_scale
            if own:
                k_seg = lax.broadcasted_iota(jnp.int32, (ROWS, ROWS), 0) // SEG
                q_seg = lax.broadcasted_iota(jnp.int32, (ROWS, ROWS), 1) // SEG
                s = jnp.where(k_seg <= q_seg, s, masked_score)
                new_max = jnp.max(s, axis=0, keepdims=True)
                w = jnp.exp2(s - new_max)
                sm_sum[h] = jnp.sum(w, axis=0, keepdims=True)
                sm_acc[h] = dot(vals, w.astype(BF16))
            else:
                old = sm_max[h]
                new_max = jnp.maximum(old, jnp.max(s, axis=0, keepdims=True))
                w = jnp.exp2(s - new_max)
                factor = jnp.exp2(old - new_max)
                sm_sum[h] = sm_sum[h] * factor + jnp.sum(w, axis=0, keepdims=True)
                sm_acc[h] = sm_acc[h] * factor + dot(vals, w.astype(BF16))
            sm_max[h] = new_max
            return 0

        lax.fori_loop(0, 2, one_head, 0)

    def z_step(step, both):
        slot_a = (z + N_SP - step) % N_SP
        slot_b = (z + step) % N_SP
        for h in range(2):
            z_copy(0, step - 1, h, slot_a).wait_recv()
            if both:
                z_copy(0, step, h, slot_a).start()
                z_copy(1, step - 1, h, slot_b).wait_recv()

                @pl.when(step < N_SP // 2 - 1)
                def _():
                    z_copy(1, step, h, slot_b).start()

    def z_attend(step, both):
        slot_a = (z + N_SP - step) % N_SP
        slot_b = (z + step) % N_SP

        @pl.when(z >= step)
        def _():
            attend(slot_a, False)

        if both:

            @pl.when(z + step >= N_SP)
            def _():
                attend(slot_b, False)

    def after_load(*which):
        for i in which:
            loads[i].wait()

    after_load(0)
    y_send(0)
    after_load(2, 3)
    y_send(1)

    after_load(1)
    own = tok[...].astype(F32)
    inv = lax.rsqrt(jnp.mean(own * own, axis=1, keepdims=True) + epsilon)
    nrm[...] = (own * inv * mix_gain[...]).astype(BF16)

    y_forward(0)
    after_load(4)
    y_send(2)
    rope_rows = dot(nrm[...], rope_weight[...])
    rope_t = jnp.concatenate([rope_rows, jnp.zeros((ROWS, 96), F32)], axis=1).T[:QK_ROPE]
    rope_t = rope_t.astype(BF16).astype(F32)
    y_finish(0)
    acc = jnp.zeros((ROWS, 128), F32)
    for g in range(N_FS):
        w = MD[g]
        left = dot(nrm[:, g * 512 : g * 512 + 256], w)
        right = dot(nrm[:, g * 512 + 256 : g * 512 + 512], w)
        acc = acc + jnp.concatenate([left[:, :64], right[:, 64:]], axis=1)
    acc_t = acc.T
    LM[t] = (acc_t[:64] + acc_t[64:]).astype(BF16)
    tp_send(0, LM)

    y_forward(1)
    after_load(5)
    y_send(3)

    cosine, sine = tables[:16], tables[16:]
    y_finish(1)
    tp_wait(0, LM)
    mem = LM[...].reshape(KV_LAT, ROWS).astype(F32)
    mem_inv = lax.rsqrt(jnp.mean(mem * mem, axis=0, keepdims=True) + epsilon)
    mem_n = (mem * mem_inv * column(memory_gain[...], ROWS)).astype(BF16)
    both_up = dot(KVU[...].reshape(KV_LAT, 256), mem_n, (0, 0))
    k_gain = column(key_gain[...], ROWS)
    rope_sq = jnp.sum(rope_t * rope_t, axis=0, keepdims=True)
    rope_g = turned(rope_t * k_gain[QK_NOPE:QK_DIM], cosine, sine)
    for h in range(2):
        nope = both_up[h * 64 : h * 64 + 64]
        mean = (jnp.sum(nope * nope, axis=0, keepdims=True) + rope_sq) * (1.0 / QK_DIM)
        k_inv = lax.rsqrt(mean + epsilon)
        KV[z, h * HEAD_ROWS : h * HEAD_ROWS + QK_NOPE] = (nope * k_inv * k_gain[:QK_NOPE]).astype(BF16)
        KV[z, h * HEAD_ROWS + QK_NOPE : h * HEAD_ROWS + QK_DIM] = (rope_g * k_inv).astype(BF16)
        KV[z, h * HEAD_ROWS + QK_DIM : (h + 1) * HEAD_ROWS] = both_up[
            128 + h * 64 : 192 + h * 64
        ].astype(BF16)
    for h in range(2):
        z_copy(0, 0, h, z).start()
        z_copy(1, 0, h, z).start()

    y_forward(2)
    after_load(6, 7)
    y_send(4)
    y_finish(2)
    acc = jnp.zeros((ROWS, 96), F32)
    for g in range(N_FS):
        acc = acc + dot(nrm[:, g * 512 : g * 512 + 512], QD[g])
    acc_t = jnp.concatenate([acc, jnp.zeros((ROWS, 32), F32)], axis=1).T
    LQ[t] = acc_t[:96].astype(BF16)
    tp_send(1, LQ)
    y_forward(3)
    after_load(8, 9)

    z_step(1, True)
    y_finish(3)
    tp_wait(1, LQ)
    lat = LQ[...].reshape(Q_LAT, ROWS).astype(F32)
    lat_inv = lax.rsqrt(jnp.mean(lat * lat, axis=0, keepdims=True) + epsilon)
    lat_n = (lat * lat_inv * column(latent_gain[...], ROWS)).astype(BF16)
    q_all = dot(QU[...].reshape(Q_LAT, 192), lat_n, (0, 0))
    q_gain = column(query_gain[...], ROWS)
    for h in range(2):
        q = q_all[h * QK_DIM : (h + 1) * QK_DIM]
        q = q * lax.rsqrt(jnp.mean(q * q, axis=0, keepdims=True) + epsilon) * q_gain[:QK_DIM]
        qt[h, :QK_NOPE] = q[:QK_NOPE].astype(BF16)
        qt[h, QK_NOPE:] = turned(q[QK_NOPE:], cosine, sine).astype(BF16)
    attend(z, True)
    z_attend(1, True)

    z_step(2, True)
    y_forward(4)
    y_send(5)
    z_attend(2, True)

    z_step(3, True)
    z_attend(3, True)
    y_finish(4)
    gates = jnp.zeros((ROWS, 256), F32)
    for g in range(N_FS):
        gates = gates + dot(nrm[:, g * 512 : g * 512 + 512], CV[g])
    gated = (gates[:, :128] * jax.nn.sigmoid(gates[:, 128:])).astype(BF16)
    ext[32:, :] = gated.astype(F32)
    halo[0] = gated[ROWS - 32 :]
    halo_copy = remote(halo.at[0], halo.at[1], hs, hr, sp=ahead)
    halo_copy.start()

    z_step(4, True)
    y_forward(5)
    z_attend(4, True)

    halo_copy.wait_recv()
    ext[:32, :] = jnp.where(z > 0, halo[1].astype(F32), 0.0)
    taps = conv_kernel[...].astype(F32)
    sums = jnp.zeros((ROWS, 128), F32)
    for j in range(CONV_K):
        sums = sums + ext[2 + j : 2 + j + ROWS, :] * taps[j : j + 1]
    conv = sums.T
    own_mean = jnp.mean(conv, axis=0, keepdims=True)
    off = conv - own_mean
    own_m2 = jnp.sum(off * off, axis=0, keepdims=True)
    stat[t] = jnp.concatenate([own_mean, own_m2, jnp.zeros((6, ROWS), F32)], axis=0)
    cmix[...] = conv
    tp_send(2, stat)

    z_step(5, True)
    z_attend(5, True)

    tp_wait(2, stat)
    means = stat[:, 0, :]
    m2 = stat[:, 1, :]
    row_mean = jnp.mean(means, axis=0, keepdims=True)
    drift = means - row_mean
    spread = jnp.sum(m2 + 128.0 * drift * drift, axis=0, keepdims=True) * (1.0 / CONV_W)
    v = (cmix[...] - row_mean) * lax.rsqrt(spread + epsilon)
    v = v * column(channel_gain[...], ROWS) + column(channel_shift[...], ROWS)
    cmix[...] = v / (1.0 + jnp.exp(-v))

    z_step(6, True)
    y_finish(5)
    z_attend(6, True)
    z_step(7, True)
    z_attend(7, True)
    z_step(8, False)
    z_attend(8, False)

    mixed = [(sm_acc[h] / sm_sum[h]) for h in range(2)]
    mix_rows = jnp.concatenate(mixed + [cmix[...]], axis=0).T.astype(BF16)
    for g in range(N_FS):
        block = dot(mix_rows, HC[g]).astype(BF16)
        part[:, :, :, g * 512 : g * 512 + 512] = block.reshape(2, 4, 32, 512)
    partner = t + 1 - 2 * core
    pair_copy = remote(part.at[1 - core], pair_in, ds.at[0], dr.at[0], tp=partner)
    pair_copy.start()
    pair_copy.wait_recv()

    near = x + 1 - 2 * (x % 2)
    across = 3 - x
    cols = (pl.ds(0, 1024), pl.ds(1024, 1024))
    first = (near, across)
    second = (across, near)

    def other(g, s):
        return g + 1 - 2 * (g % 2) if s == 0 else 3 - g

    total[...] = (part[core].astype(F32) + pair_in[...].astype(F32)).astype(BF16)

    def halve1(s, k):
        g = first[s] if k == 0 else other(first[s], 1 - s)
        return remote(
            total.at[g, :, cols[s]], r1.at[s, k], xs.at[0, s, k], xr.at[0, s, k], tp=2 * first[s] + core
        )

    for k in (1, 0):
        for s in range(2):
            halve1(s, k).start()
    for s in range(2):
        halve1(s, 1).wait_recv()
        g = second[s]
        s2[s] = (total[g, :, s * 1024 : (s + 1) * 1024].astype(F32) + r1[s, 1].astype(F32)).astype(BF16)

        def halve2(s=s):
            return remote(s2.at[s], r2.at[s], xs.at[1, s, 0], xr.at[1, s, 0], tp=2 * second[s] + core)

        halve2().start()

    def out_piece(c, g, s):
        return outv.at[c, g, :, cols[s]]

    def gather1(s, g):
        p = out_piece(core, g, s)
        return remote(p, p, xs.at[2, s, 0], xr.at[2, s, 0], tp=2 * second[s] + core)

    def gather2(s, k, g):
        p = out_piece(core, g, s)
        return remote(p, p, xs.at[3, s, k], xr.at[3, s, k], tp=2 * first[s] + core)

    def to_pair(s, k, c, g):
        p = out_piece(c, g, s)
        return remote(p, p, ds.at[1 + s * 4 + k], dr.at[1 + s * 4 + k], tp=partner)

    for s in range(2):
        halve1(s, 0).wait_recv()
        remote(
            s2.at[s], r2.at[s], xs.at[1, s, 0], xr.at[1, s, 0], tp=2 * second[s] + core
        ).wait_recv()
        mine = (
            total[x, :, s * 1024 : (s + 1) * 1024].astype(F32)
            + r1[s, 0].astype(F32)
            + r2[s].astype(F32)
        )
        outv[core, x, :, s * 1024 : (s + 1) * 1024] = mine.astype(BF16)
        gather1(s, x).start()
        gather2(s, 0, x).start()
        to_pair(s, 0, core, x).start()
    for s in range(2):
        gather1(s, second[s]).wait_recv()
        gather2(s, 1, second[s]).start()
        to_pair(s, 1, core, second[s]).start()
    for s in range(2):
        g0, g1 = first[s], other(first[s], 1 - s)
        gather2(s, 0, g0).wait_recv()
        to_pair(s, 2, core, g0).start()
        gather2(s, 1, g1).wait_recv()
        to_pair(s, 3, core, g1).start()
    for s in range(2):
        groups = (x, second[s], first[s], other(first[s], 1 - s))
        for k in range(4):
            to_pair(s, k, 1 - core, groups[k]).wait_recv()
    copies = []
    for c in range(2):
        for g in range(4):
            copy = pltpu.make_async_copy(
                outv.at[c, g], out_h.at[0, pl.ds(c * 128 + g * 32, 32)], out_sem.at[c, g]
            )
            copy.start()
            copies.append(copy)
    for copy in copies:
        copy.wait()

    for i in range(len(weights)):
        for copy in y_copies(i)[:4]:
            copy.wait_send()
    for k, buf in ((0, LM), (1, LQ), (2, stat)):

        def sent(d, _, k=k, buf=buf):
            remote(buf.at[t], buf.at[t], ts.at[k, d], tr.at[k, d], tp=(t + d) % N_TP).wait_send()
            return 0

        lax.fori_loop(1, N_TP, sent, 0)

    def z_sent(step, _):
        for h in range(2):
            z_copy(0, step, h, (z + N_SP - step) % N_SP).wait_send()

            @pl.when(step < N_SP // 2 - 1)
            def _():
                z_copy(1, step, h, (z + step) % N_SP).wait_send()

        return 0

    lax.fori_loop(0, N_SP // 2, z_sent, 0)
    halo_copy.wait_send()
    pair_copy.wait_send()
    for s in range(2):
        for k in range(2):
            halve1(s, k).wait_send()
        remote(s2.at[s], r2.at[s], xs.at[1, s, 0], xr.at[1, s, 0], tp=2 * second[s] + core).wait_send()
        gather1(s, x).wait_send()
        gather2(s, 0, x).wait_send()
        gather2(s, 1, second[s]).wait_send()
        groups = (x, second[s], first[s], other(first[s], 1 - s))
        for k in range(4):
            to_pair(s, k, core, groups[k]).wait_send()


def local(
    tokens, mix_gain, query_down, memory_down, rope_weight, query_up, key_up, value_up,
    latent_gain, memory_gain, query_gain, key_gain, conv_value, conv_gate, conv_kernel,
    channel_gain, channel_shift, heads_out, conv_out,
):
    memory_pairs = jnp.concatenate([memory_down[:256], memory_down[256:]], axis=1)
    positions = (lax.axis_index("sp") * ROWS + jnp.arange(ROWS, dtype=jnp.int32)).astype(F32)
    inverse_freq = 1.0 / rope_base ** (jnp.arange(0, QK_ROPE, 2, dtype=F32) / QK_ROPE)
    angles = inverse_freq[:, None] * positions[None, :]
    tables = jnp.concatenate([jnp.cos(angles), jnp.sin(angles)], axis=0)

    def row(v):
        v = v.reshape(1, -1)
        return jnp.pad(v, ((0, 0), (0, -v.shape[1] % 128)))

    hbm = pl.BlockSpec(memory_space=pl.ANY)
    vmem = pl.BlockSpec(memory_space=pltpu.VMEM)
    dma = pltpu.SemaphoreType.DMA
    return pl.pallas_call(
        kernel,
        out_shape=jax.ShapeDtypeStruct((1, ROWS, D), BF16),
        in_specs=[hbm] * 10 + [vmem] * 10,
        out_specs=hbm,
        scratch_shapes=[
            pltpu.VMEM((ROWS, D), BF16),
            pltpu.VMEM((ROWS, D), BF16),
            pltpu.VMEM((N_FS, 256, 128), BF16),
            pltpu.VMEM((N_FS, 128, 256), BF16),
            pltpu.VMEM((N_FS, 512, 96), BF16),
            pltpu.VMEM((N_FS, 192, 192), BF16),
            pltpu.VMEM((N_FS, 512, 256), BF16),
            pltpu.VMEM((N_FS, 256, 512), BF16),
            pltpu.VMEM((N_TP, 64, ROWS), BF16),
            pltpu.VMEM((N_TP, 96, ROWS), BF16),
            pltpu.VMEM((N_SP, 2 * HEAD_ROWS, ROWS), BF16),
            pltpu.VMEM((2, QK_DIM, ROWS), BF16),
            pltpu.VMEM((N_TP, 8, ROWS), F32),
            pltpu.VMEM((2, 32, 128), BF16),
            pltpu.VMEM((ROWS + 32, 128), F32),
            pltpu.VMEM((128, ROWS), F32),
            pltpu.VMEM((2, 1, ROWS), F32),
            pltpu.VMEM((2, 1, ROWS), F32),
            pltpu.VMEM((2, V_DIM, ROWS), F32),
            pltpu.VMEM((2, 4, 32, D), BF16),
            pltpu.VMEM((4, 32, D), BF16),
            pltpu.VMEM((4, 32, D), BF16),
            pltpu.VMEM((2, 2, 32, 1024), BF16),
            pltpu.VMEM((2, 32, 1024), BF16),
            pltpu.VMEM((2, 32, 1024), BF16),
            pltpu.VMEM((2, 4, 32, D), BF16),
            dma((10,)),
            dma((6, 4)),
            dma((6, 4)),
            dma((3, N_TP)),
            dma((3, N_TP)),
            dma((2, N_SP // 2, 2)),
            dma((2, N_SP // 2, 2)),
            dma,
            dma,
            dma((9,)),
            dma((9,)),
            dma((4, 2, 2)),
            dma((4, 2, 2)),
            dma((2, 4)),
        ],
        compiler_params=pltpu.CompilerParams(
            collective_id=0, has_side_effects=True, vmem_limit_bytes=40 * 1024 * 1024
        ),
        name="layer",
    )(
        tokens, memory_pairs, query_down, query_up, key_up, value_up, conv_value, conv_gate,
        heads_out, conv_out,
        row(mix_gain), rope_weight, row(latent_gain), row(memory_gain), row(query_gain),
        row(key_gain), conv_kernel, row(channel_gain), row(channel_shift), tables,
    )


def solution(mesh):
    in_specs = (
        P("fs", "sp", None),
        P(),
        P("fs", "tp"),
        P("fs", "tp"),
        P(),
        P("fs", "tp"),
        P("fs", "tp"),
        P("fs", "tp"),
        P(),
        P(),
        P(),
        P(),
        P("fs", "tp"),
        P("fs", "tp"),
        P(None, "tp"),
        P("tp"),
        P("tp"),
        P("tp", "fs"),
        P("tp", "fs"),
    )
    out_specs = P("fs", "sp", None)
    return jax.shard_map(local, mesh=mesh, in_specs=in_specs, out_specs=out_specs, check_vma=False)
```

time: 268 us -> 103 us (0.38)
  waiting for transfers between devices: 131 us -> 0 us
  Pallas kernels: 0 us -> 92.5 us
  other arithmetic: 46.1 us -> 0.26 us
  blocking collectives: 34.5 us -> 0 us
  matrix products: 13.8 us -> 0 us
  between operations: 13.6 us -> 0.2 us
  local copies, waits for them, and re-layouts: 19.8 us -> 9.57 us
  starting transfers between devices: 7.13 us -> 0 us
    all_gather x4 -> x0, waiting for transfers between devices: 126 us -> none  [the longest x3 65.6 us: side_by_side(): lax.all_gather(both, axis, axis=dim, tiled=True)]
    pallas_call x0 -> x1, Pallas kernels: none -> 92.5 us  [local(): pl.pallas_call(kernel, out_shape=jax.ShapeDtypeStruct((1, ROWS, D), BF16)...]
    all_gather x3 -> x0, blocking collectives: 34.5 us -> none  [the longest x1 13.9 us: one_gather(): lines, at, outs = (lax.all_gather(vector, axis), 0, [])]
    mul x33 -> x0, other arithmetic: 22.4 us -> none  [the longest x31 21.5 us: add_tap(): return running + window * weight_row]
    reduce_sum x9 -> x0, other arithmetic: 14.1 us -> none  [the longest x2 6.89 us: attend(): row_total = row_total * factor + jnp.sum(weights, axis=2)]
    dot_general x9 -> x0, matrix products: 13.8 us -> none  [the longest x2 5.67 us: attend(): jnp.einsum('qhd,khd->qhk', queries, key_rows, preferred_element_type=jnp....]
    dynamic_slice x66 -> x0, local copies, waits for them, and re-layouts: 6.55 us -> none  [the longest x62 6.35 us: add_tap(): lax.dynamic_slice_in_dim(extended, tap_index, row_count, 0)]
    concatenate x9 -> x2, other arithmetic: 5.28 us -> 0.1 us  [the longest x1 0.1 us: local(): jnp.concatenate([memory_down[:256], memory_down[256:]], axis=1)]
  transfers between devices with their start and end apart: 6 -> 0, of which waited for: 5 -> 0; matrix products, arithmetic and copies ran while one was open for 21% -> 0% of each run, Pallas kernels for 0% -> 0%
where the time goes in v1:
time: 103 us
  Pallas kernels  92.5 us (90%)
  local copies, waits for them, and re-layouts  9.57 us (9%)
    pallas_call x1, Pallas kernels, local(): pl.pallas_call(kernel, out_shape=jax.ShapeDtypeStruct((1, ROWS, D), BF16)...  92.5 us
    unnamed x31, local copies, waits for them, and re-layouts  6.68 us

profile of v1, /device:TPU:1, one launch (start us, length us, event | category | flops | bytes accessed | tf_op | source)
XLA Modules:
  0.0 102.5 jit_solution(14728935272785077321)
XLA Ops:
  0.0 0.7 pad.7.query_gain
  0.8 0.7 pad.8.key_gain
  1.4 0.7 reshape.33.latent_gain
  2.1 0.1 multiply_cosine_fusion
  2.3 0.8 fusion
  3.1 0.1 copy.24
  3.2 0.1 copy.25
  3.3 0.1 pad_maximum_fusion.md_h
  3.4 1.0 copy.22.qd_h
  4.4 0.0 copy-start.1
  4.4 0.0 copy-start.2
  4.4 0.0 copy-start.3
  4.5 0.0 copy-start.5
  4.5 0.0 copy-start.8
  4.5 0.0 copy-start.10
  4.5 0.0 copy-start.11
  4.5 0.0 copy-start.12
  4.5 1.3 %copy.23.rope_weight = bf16[2048,32]{1,0:T(8,128)(2,1)S(1)} copy(bf16[2048,32]{0,1:T(8,128)(2,1)} %param.23) | data formatting | bytes 262144 | tf_op args[4]
  5.8 0.0 copy-done
  5.8 0.0 copy-done.1
  5.8 0.0 copy-done.2
  5.9 0.0 copy-done.3
  5.9 0.0 copy-done.5
  5.9 0.0 copy-done.8
  5.9 0.0 copy-done.10
  5.9 0.0 copy-start.4
  5.9 0.9 copy-done.4
  6.8 0.8 copy-done.6
  7.6 0.8 copy-done.7
  8.3 0.7 copy-done.9
  9.0 92.5 %layer.1 = bf16[1,256,2048]{2,1,0:T(8,128)(2,1)S(1)} custom-call(bf16[1,256,2048]{2,1,0:T(8,128)(2,1)S(1)} %copy-done, bf16[256,128]{1,0:T(8,128)(2,1)S(1)} %pad_maximum_fusion.md_h, bf16[512,96]{1,0:T(8,128)(2,1)S(1)} %copy.22.qd_h, bf16[192,192]{1,0:T(8,128)(2,1)S(1)} %copy-done.5, bf16[128,128]{1,0:T(8,128)(2,1)S(1)} %copy-done.6, ...), custom_call_target="tpu_custom_call" | custom-call | tf_op jit(solution)/shard_map/layer/pallas_call | solution.py:514
  101.5 1.0 copy.27
  (9 shorter events, 0.0 us)
Async XLA Ops:
  0.0 5.8 %copy-start = (bf16[1,256,2048]{2,1,0:T(8,128)(2,1)S(1)}, bf16[1,256,2048]{2,1,0:T(8,128)(2,1)}, u32[]{:S(2)}) copy-start(bf16[1,256,2048]{2,1,0:T(8,128)(2,1)} %tokens_h.1) | copy-start | bytes 3145732
  4.4 1.4 %copy-start.1 = (bf16[512,128]{1,0:T(8,128)(2,1)S(1)}, bf16[512,128]{1,0:T(8,128)(2,1)}, u32[]{:S(2)}) copy-start(bf16[512,128]{1,0:T(8,128)(2,1)} %cv_h.1) | copy-start | bytes 393220
  4.4 1.4 %copy-start.2 = (bf16[512,128]{1,0:T(8,128)(2,1)S(1)}, bf16[512,128]{1,0:T(8,128)(2,1)}, u32[]{:S(2)}) copy-start(bf16[512,128]{1,0:T(8,128)(2,1)} %cg_h.1) | copy-start | bytes 393220
  4.4 1.4 %copy-start.3 = (bf16[128,512]{1,0:T(8,128)(2,1)S(1)}, bf16[128,512]{1,0:T(8,128)(2,1)}, u32[]{:S(2)}) copy-start(bf16[128,512]{1,0:T(8,128)(2,1)} %ho_h.1) | copy-start | bytes 393220
  4.5 1.4 %copy-start.5 = (bf16[192,192]{1,0:T(8,128)(2,1)S(1)}, bf16[192,192]{1,0:T(8,128)(2,1)}, u32[]{:S(2)}) copy-start(bf16[192,192]{1,0:T(8,128)(2,1)} %qu_h.1) | copy-start | bytes 221188
  4.5 1.4 %copy-start.8 = (f32[2048]{0:T(1024)S(1)}, f32[2048]{0:T(1024)}, u32[]{:S(2)}) copy-start(f32[2048]{0:T(1024)} %param.20) | copy-start | bytes 24580
  4.5 1.4 %copy-start.10 = (f32[512]{0:T(512)S(1)}, f32[512]{0:T(512)}, u32[]{:S(2)}) copy-start(f32[512]{0:T(512)} %param.28) | copy-start | bytes 6148
  4.5 1.4 %copy-start.11 = (f32[128]{0:T(128)S(1)}, f32[128]{0:T(128)}, u32[]{:S(2)}) copy-start(f32[128]{0:T(128)} %param.34) | copy-start | bytes 1540
  4.5 1.4 %copy-start.12 = (f32[128]{0:T(128)S(1)}, f32[128]{0:T(128)}, u32[]{:S(2)}) copy-start(f32[128]{0:T(128)} %param.35) | copy-start | bytes 1540
  5.9 0.9 copy-start.4
  6.8 0.8 copy-start.6
  7.6 0.8 copy-start.7
  8.3 0.7 copy-start.9
